TPU v7x, 512 devices: a whole 4x4x16 slice. The times are simulated.
512 devices in a mesh: fs: 16 (over y, x), tp: 32 (over z, core).
Axes of the slice: x: 4, y: 4, z: 16, core: 2. Of those that a mesh axis runs over, the one named last changes fastest.
Arguments:
- saved_input: bfloat16 [16384, 4096], P('fs', 'tp'), may hold values from -6 to 6
- query_cot: bfloat16 [16384, 4096], P('fs', 'tp'), may hold values from -6 to 6
- key_cot: bfloat16 [16384, 4096], P('fs', 'tp'), may hold values from -6 to 6
- query_master: float32 [4096, 4096], P('fs', 'tp'), may hold values from -0.09375 to 0.09375
- key_master: float32 [4096, 4096], P('fs', 'tp'), may hold values from -0.09375 to 0.09375
- query_basis: bfloat16 [4096, 256], P('fs'), may hold values from -3 to 3
- key_basis: bfloat16 [4096, 256], P('fs'), may hold values from -3 to 3
- query_first: float32 [256, 4096], P('fs', 'tp'), may hold values from -240 to 240
- query_second: float32 [256, 4096], P('fs', 'tp'), may hold values from 1000 to 20000
- key_first: float32 [256, 4096], P('fs', 'tp'), may hold values from -240 to 240
- key_second: float32 [256, 4096], P('fs', 'tp'), may hold values from 1000 to 20000
Outputs:
- query_step: float32 [4096, 4096], P('fs', 'tp')
- query_weight: float32 [4096, 4096], P('fs', 'tp')
- query_copy: bfloat16 [4096, 4096], P(None, 'tp')
- query_first_new: float32 [256, 4096], P('fs', 'tp')
- query_second_new: float32 [256, 4096], P('fs', 'tp')
- key_step: float32 [4096, 4096], P('fs', 'tp')
- key_weight: float32 [4096, 4096], P('fs', 'tp')
- key_copy: bfloat16 [4096, 4096], P(None, 'tp')
- key_first_new: float32 [256, 4096], P('fs', 'tp')
- key_second_new: float32 [256, 4096], P('fs', 'tp')
All inputs are finite; a program needn't handle non-finite values.
Results may differ from a plain program's by a relative error of at most 0.0065.
Values may be sent and summed in bfloat16 or wider, within the bound.
A program may use at most 64 MiB of HBM per device.

v0:
```python
import jax
import jax.numpy as jnp
from jax import lax
from jax.sharding import Mesh
from jax.sharding import PartitionSpec as P

D = 4096
HD = 128
FS = ("fs_0", "fs_1")
moment_decay = 0.8
square_decay = 0.9
square_floor = 1.0
norm_floor = 0.01
step_rate = 0.01


def in_one_piece(arrays, axis, dim, along):
    widths = [a.shape[along] for a in arrays]
    both = jnp.concatenate(arrays, axis=along)
    out = lax.all_gather(both, axis, axis=dim, tiled=True)
    return tuple(jnp.split(out, [sum(widths[:k]) for k in range(1, len(widths))], axis=along))


def cut_along(x, dim, count):
    lengths = x.shape
    pieces = x.reshape(*lengths[:dim], count, lengths[dim] // count, *lengths[dim + 1 :])
    return jnp.moveaxis(pieces, dim, 0)


def sent_and_summed(x, axis, dim):
    count = lax.axis_size(axis)
    pieces = lax.all_to_all(cut_along(x, dim, count), axis, 0, 0, tiled=True)
    return jnp.sum(pieces, axis=0)


def sent_to_all(x, axis):
    count = lax.axis_size(axis)
    return lax.all_to_all(jnp.broadcast_to(x[None], (count, *x.shape)), axis, 0, 0, tiled=True)


def in_order(pieces, dim):
    lengths = list(pieces.shape[1:])
    lengths[dim] *= pieces.shape[0]
    return jnp.moveaxis(pieces, 0, dim).reshape(lengths)


def gathered_copies(x, axis, dim):
    pieces = sent_to_all(x, axis)
    return in_order(pieces, dim)


def by_axis(x, axes):
    for axis in axes:
        x = lax.psum(x, axis)
    return x


def split_product(low_part, cot_part):
    upper = low_part.astype(jnp.bfloat16)
    lower = (low_part - upper.astype(jnp.float32)).astype(jnp.bfloat16)
    return jnp.dot(upper.T, cot_part, preferred_element_type=jnp.float32) + jnp.dot(
        lower.T, cot_part, preferred_element_type=jnp.float32
    )


def cot_rows(query_low, key_low, cot_wide, width):

    def low_rows(start, count):
        return jnp.concatenate(
            [
                split_product(query_low, cot_wide[:, :width]),
                split_product(key_low, cot_wide[:, width:]),
            ],
            axis=1,
        )

    return low_rows


def head_squares(update):
    by_head = update.reshape(update.shape[0], -1, HD)
    return jnp.sum(by_head * by_head, axis=(0, 2))


def apply_scale(update, total):
    scale = 1.0 / jnp.sqrt(total / (D * HD) + norm_floor)
    by_head = update.reshape(update.shape[0], -1, HD)
    return (by_head * scale[None, :, None]).reshape(update.shape)


def body(
    saved_input,
    query_cot,
    key_cot,
    query_master,
    key_master,
    query_basis,
    key_basis,
    query_first,
    query_second,
    key_first,
    key_second,
):
    width = query_cot.shape[1]
    low_count = query_first.shape[0]
    cotangents = jnp.concatenate([query_cot, key_cot], axis=1)
    inputs = lax.all_gather(saved_input, "tp", axis=1, tiled=True)
    bases = in_one_piece((query_basis, key_basis), FS, 0, 1)
    query_low = jnp.dot(inputs, bases[0], preferred_element_type=jnp.float32)
    key_low = jnp.dot(inputs, bases[1], preferred_element_type=jnp.float32)
    low_rows = cot_rows(query_low, key_low, cotangents, width)
    projected = sent_and_summed(low_rows(jnp.int32(0), low_count * lax.axis_size(FS)), FS, 0)
    firsts = jnp.concatenate([query_first, key_first], axis=1)
    seconds = jnp.concatenate([query_second, key_second], axis=1)
    first_new = moment_decay * firsts + (1.0 - moment_decay) * projected
    second_new = square_decay * seconds + (1.0 - square_decay) * projected * projected
    ratio = (first_new / jnp.sqrt(second_new + square_floor)).astype(jnp.bfloat16)
    piece = gathered_copies(ratio, FS, 0)
    query_update = jnp.dot(query_basis, piece[:, :width], preferred_element_type=jnp.float32)
    key_update = jnp.dot(key_basis, piece[:, width:], preferred_element_type=jnp.float32)
    query_total, key_total = (
        by_axis(head_squares(query_update), FS),
        by_axis(head_squares(key_update), FS),
    )
    query_step = apply_scale(query_update, query_total)
    key_step = apply_scale(key_update, key_total)
    query_weight = query_master - step_rate * query_step
    key_weight = key_master - step_rate * key_step
    copies = in_one_piece(
        (query_weight.astype(jnp.bfloat16), key_weight.astype(jnp.bfloat16)), FS, 0, 1
    )
    return (
        query_step,
        query_weight,
        copies[0],
        first_new[:, :width],
        second_new[:, :width],
        key_step,
        key_weight,
        copies[1],
        first_new[:, width:],
        second_new[:, width:],
    )


def solution(mesh):
    torus = Mesh(mesh.devices.reshape(4, 4, mesh.shape["tp"]), ("fs_0", "fs_1", "tp"))
    in_specs = (
        P(FS, "tp"),
        P(FS, "tp"),
        P(FS, "tp"),
        P(FS, "tp"),
        P(FS, "tp"),
        P(FS, None),
        P(FS, None),
        P(FS, "tp"),
        P(FS, "tp"),
        P(FS, "tp"),
        P(FS, "tp"),
    )
    out_specs = (
        P(FS, "tp"),
        P(FS, "tp"),
        P(None, "tp"),
        P(FS, "tp"),
        P(FS, "tp"),
        P(FS, "tp"),
        P(FS, "tp"),
        P(None, "tp"),
        P(FS, "tp"),
        P(FS, "tp"),
    )
    return jax.shard_map(body, mesh=torus, in_specs=in_specs, out_specs=out_specs, check_vma=False)
```

profile of v0, /device:TPU:2, one launch (start us, length us, event | category | flops | bytes accessed | tf_op | source)
XLA Modules:
  0.0 306.8 jit_solution(4869370095504522026)
XLA Ops:
  7.2 1.7 pad_maximum_fusion
  9.0 0.7 all-gather.6.cloned.1.call-update
  9.7 73.1 %all-gather.4.cloned.1.call-done = bf16[4096,512]{1,0:T(8,128)(2,1)} async-done(((bf16[256,512]{1,0:T(8,128)(2,1)}), bf16[4096,512]{1,0:T(8,128)(2,1)}) %all-gather.4.cloned.1.call-update) | async-done | bytes 4194320 | tf_op jit(solution)/shard_map/all_gather | solution.py:20
  82.8 97.5 %all-gather.6.cloned.1.call-done = bf16[1024,4096]{1,0:T(8,128)(2,1)} async-done(((bf16[1024,128]{1,0:T(8,128)(2,1)}), bf16[1024,4096]{1,0:T(8,128)(2,1)}) %all-gather.6.cloned.1.call-update) | async-done | bytes 8388624 | tf_op jit(solution)/shard_map/all_gather | solution.py:107
  180.2 6.5 %fusion.4 = f32[1024,256]{0,1:T(8,128)S(1)} fusion(bf16[1024,4096]{1,0:T(8,128)(2,1)} %all-gather.6.cloned.1.call-done, bf16[4096,512]{1,0:T(8,128)(2,1)} %all-gather.4.cloned.1.call-done), kind=kOutput, calls=%fused_computation.4 | convolution fusion | flops 2147483648 | bytes 11534336 | tf_op jit(solution)/shard_map/dot_general | solution.py:109
  187.8 2.4 fusion.7
  191.1 14.8 %all_to_all.10 = f32[16,16,256]{2,1,0:T(8,128)S(1)} all-to-all(f32[16,16,256]{2,1,0:T(8,128)S(1)} %bitcast.24), channel_id=1, replica_groups=mesh['fs_0'=4,'fs_1'=4,'tp'=32] {'fs_0','fs_1'}, dimensions={0} | all-to-all | bytes 524288 | tf_op jit(solution)/shard_map/all_to_all | solution.py:32
  206.0 0.7 broadcast_in_dim.2
  206.7 4.8 %all-to-all-start.1 = ((bf16[16,16,256]{2,1,0:T(8,128)(2,1)}), bf16[16,16,256]{2,1,0:T(8,128)(2,1)S(1)}, u32[]{:S(2)}, u32[]{:S(2)}) async-start(bf16[16,16,256]{2,1,0:T(8,128)(2,1)} %broadcast_in_dim.2), calls=%async_computation.1 | async-start | bytes 262144 | tf_op jit(solution)/shard_map/all_to_all | solution.py:38
  211.7 6.4 %all-to-all-done.1 = bf16[16,16,256]{2,1,0:T(8,128)(2,1)S(1)} async-done(((bf16[16,16,256]{2,1,0:T(8,128)(2,1)}), bf16[16,16,256]{2,1,0:T(8,128)(2,1)S(1)}, u32[]{:S(2)}, u32[]{:S(2)}) %all-to-all-start.1) | async-done | bytes 131104 | tf_op jit(solution)/shard_map/all_to_all | solution.py:38
  218.2 0.8 multiply_reduce_fusion.1
  219.0 0.8 multiply_reduce_fusion
  219.8 9.2 %all-reduce.1 = (f32[1]{0:T(128)}, f32[1]{0:T(128)}) all-reduce(f32[1]{0:T(128)} %bitcast.4, f32[1]{0:T(128)} %bitcast.7), channel_id=1, replica_groups=mesh['fs_0'=4,'fs_1'=4,'tp'=32] {'fs_0'}, use_global_device_ids=true, to_apply=%region_2.0 | all-reduce | flops 2 | bytes 16 | tf_op jit(solution)/shard_map/psum | solution.py:54
  229.0 9.8 %all-reduce = (f32[1]{0:T(128)}, f32[1]{0:T(128)}) all-reduce(f32[1]{0:T(128)} %get-tuple-element.32, f32[1]{0:T(128)} %get-tuple-element.33), channel_id=1, replica_groups=mesh['fs_0'=4,'fs_1'=4,'tp'=32] {'fs_1'}, use_global_device_ids=true, to_apply=%region_3.0 | all-reduce | flops 2 | bytes 16 | tf_op jit(solution)/shard_map/psum | solution.py:54
  240.2 0.7 pad_maximum_fusion.2
  240.9 0.6 fusion.27
  241.5 0.8 copy.32
  242.3 0.8 copy.33
  243.1 0.8 copy.35
  243.8 0.8 copy.36
  244.6 51.4 %all-gather.8.cloned.1.call-done = bf16[4096,256]{0,1:T(8,128)(2,1)} async-done(((bf16[256,256]{0,1:T(8,128)(2,1)}), bf16[4096,256]{0,1:T(8,128)(2,1)}) %all-gather.8.cloned.1.call-update) | async-done | bytes 2097168 | tf_op jit(solution)/shard_map/all_gather | solution.py:20
  296.0 1.7 fusion.26
  297.6 1.3 copy.34
  299.0 1.3 copy.37
  (40 shorter events, 2.3 us)
Async XLA Ops:
  7.2 179.6 %copy-start = (bf16[1024,128]{1,0:T(8,128)(2,1)S(1)}, bf16[1024,128]{1,0:T(8,128)(2,1)}, u32[]{:S(2)}) copy-start(bf16[1024,128]{1,0:T(8,128)(2,1)} %param.12) | copy-start | bytes 786436
  7.2 75.6 %all-gather.4.cloned.1.call-start = ((), (), s32[]{:S(2)}) async-start(), calls=%async_computation.2 | async-start | bytes 4456448 | tf_op jit(solution)/shard_map/all_gather | solution.py:20
  9.0 171.3 %all-gather.6.cloned.1.call-start = ((), (), s32[]{:S(2)}) async-start(), calls=%async_computation.3 | async-start | bytes 8650752 | tf_op jit(solution)/shard_map/all_gather | solution.py:107
  180.2 7.2 %copy-start.10 = (bf16[1024,4096]{1,0:T(8,128)(2,1)S(1)}, bf16[1024,4096]{1,0:T(8,128)(2,1)}, u32[]{:S(2)}) copy-start(bf16[1024,4096]{1,0:T(8,128)(2,1)} %all-gather.6.cloned.1.call-done) | copy-start | bytes 25165828
  180.2 7.6 %copy-start.11 = (bf16[4096,512]{1,0:T(8,128)(2,1)S(1)}, bf16[4096,512]{1,0:T(8,128)(2,1)}, u32[]{:S(2)}) copy-start(bf16[4096,512]{1,0:T(8,128)(2,1)} %all-gather.4.cloned.1.call-done) | copy-start | bytes 12582916
  187.8 2.4 copy-start.1
  190.2 15.7 %copy-start.6 = (f32[16,128]{1,0:T(8,128)S(1)}, f32[16,128]{1,0:T(8,128)}, u32[]{:S(2)}) copy-start(f32[16,128]{1,0:T(8,128)} %param.21) | copy-start | bytes 24580
  190.2 15.7 %copy-start.7 = (f32[16,128]{1,0:T(8,128)S(1)}, f32[16,128]{1,0:T(8,128)}, u32[]{:S(2)}) copy-start(f32[16,128]{1,0:T(8,128)} %param.19) | copy-start | bytes 24580
  190.3 15.7 %copy-start.8 = (f32[16,128]{1,0:T(8,128)S(1)}, f32[16,128]{1,0:T(8,128)}, u32[]{:S(2)}) copy-start(f32[16,128]{1,0:T(8,128)} %param.20) | copy-start | bytes 24580
  190.3 15.7 %copy-start.9 = (f32[16,128]{1,0:T(8,128)S(1)}, f32[16,128]{1,0:T(8,128)}, u32[]{:S(2)}) copy-start(f32[16,128]{1,0:T(8,128)} %param.18) | copy-start | bytes 24580
  190.3 21.2 %copy-start.4 = (f32[256,128]{1,0:T(8,128)S(1)}, f32[256,128]{1,0:T(8,128)}, u32[]{:S(2)}) copy-start(f32[256,128]{1,0:T(8,128)} %param.14) | copy-start | bytes 393220
  190.3 21.3 %copy-start.5 = (f32[256,128]{1,0:T(8,128)S(1)}, f32[256,128]{1,0:T(8,128)}, u32[]{:S(2)}) copy-start(f32[256,128]{1,0:T(8,128)} %param.15) | copy-start | bytes 393220
  190.3 27.9 %copy-start.2 = (bf16[256,256]{1,0:T(8,128)(2,1)S(1)}, bf16[256,256]{1,0:T(8,128)(2,1)}, u32[]{:S(2)}) copy-start(bf16[256,256]{1,0:T(8,128)(2,1)} %param.16) | copy-start | bytes 393220
  190.3 28.7 %copy-start.3 = (bf16[256,256]{1,0:T(8,128)(2,1)S(1)}, bf16[256,256]{1,0:T(8,128)(2,1)}, u32[]{:S(2)}) copy-start(bf16[256,256]{1,0:T(8,128)(2,1)} %param.17) | copy-start | bytes 393220
  206.7 11.5 %all-to-all-start.1 = ((bf16[16,16,256]{2,1,0:T(8,128)(2,1)}), bf16[16,16,256]{2,1,0:T(8,128)(2,1)S(1)}, u32[]{:S(2)}, u32[]{:S(2)}) async-start(bf16[16,16,256]{2,1,0:T(8,128)(2,1)} %broadcast_in_dim.2), calls=%async_computation.1 | async-start | bytes 262144 | tf_op jit(solution)/shard_map/all_to_all | solution.py:38
  211.5 84.5 %all-gather.8.cloned.1.call-start = ((), (), s32[]{:S(2)}) async-start(), calls=%async_computation.4 | async-start | bytes 2228224 | tf_op jit(solution)/shard_map/all_gather | solution.py:20
Sparse Core Ops, SparseCore 0:
  11.6 71.1 all-gather.3
  84.8 95.3 all-gather.5
  241.1 54.8 all-gather.7
where the time goes:
time: 307 us
  waiting for transfers between devices  229 us (75%)
  blocking collectives  33.8 us (11%)
  between operations  15.4 us (5%)
  matrix products  11.8 us (4%)
  local copies, waits for them, and re-layouts  9.34 us (3%)
  starting transfers between devices  4.88 us (2%)
    all_gather x2, waiting for transfers between devices, in_one_piece(): out = lax.all_gather(both, axis, axis=dim, tiled=True)  124 us
    all_gather x1, waiting for transfers between devices, body(): inputs = lax.all_gather(saved_input, 'tp', axis=1, tiled=True)  97.5 us
    psum x2, blocking collectives, by_axis(): x = lax.psum(x, axis)  19 us
    all_to_all x1, blocking collectives, sent_and_summed(): pieces = lax.all_to_all(cut_along(x, dim, count), axis, 0, 0, tiled=True)  14.8 us
    dot_general x1, matrix products, body(): query_low = jnp.dot(inputs, bases[0], preferred_element_type=jnp.float32)  6.54 us
    all_to_all x1, waiting for transfers between devices, sent_to_all(): lax.all_to_all(jnp.broadcast_to(x[None], (count, *x.shape)), axis, 0, 0,...  6.45 us
    unnamed x32, local copies, waits for them, and re-layouts  6.25 us
  transfers between devices with their start and end apart: 4, of which 4 were waited for; matrix products, arithmetic and copies ran while one was open for 1% of the time, Pallas kernels for 0%

commit v1 on v0

--- a/solution.py
+++ b/solution.py
@@ -104,7 +104,9 @@
     width = query_cot.shape[1]
     low_count = query_first.shape[0]
     cotangents = jnp.concatenate([query_cot, key_cot], axis=1)
-    inputs = lax.all_gather(saved_input, "tp", axis=1, tiled=True)
+    inputs = jnp.concatenate(
+        lax.all_to_all(jnp.stack([saved_input] * lax.axis_size("tp")), "tp", 0, 0), axis=1
+    )
     bases = in_one_piece((query_basis, key_basis), FS, 0, 1)
     query_low = jnp.dot(inputs, bases[0], preferred_element_type=jnp.float32)
     key_low = jnp.dot(inputs, bases[1], preferred_element_type=jnp.float32)

time: 307 us -> 524 us (1.71)
  waiting for transfers between devices: 229 us -> 423 us
  starting transfers between devices: 4.88 us -> 20.6 us
    all_to_all x0 -> x1, waiting for transfers between devices: none -> 289 us  [body(): lax.all_to_all(jnp.stack([saved_input] * lax.axis_size('tp')), 'tp', 0, 0)]
    all_gather x1 -> x0, waiting for transfers between devices: 97.5 us -> none  [body(): inputs = lax.all_gather(saved_input, 'tp', axis=1, tiled=True)]
    all_to_all x0 -> x1, starting transfers between devices: none -> 15.7 us  [body(): lax.all_to_all(jnp.stack([saved_input] * lax.axis_size('tp')), 'tp', 0, 0)]
where the time goes in v1:
time: 524 us
  waiting for transfers between devices  423 us (81%)
  blocking collectives  33.8 us (6%)
  starting transfers between devices  20.6 us (4%)
  between operations  15.7 us (3%)
  matrix products  15.2 us (3%)
  local copies, waits for them, and re-layouts  14.4 us (3%)
    all_to_all x1, waiting for transfers between devices, body(): lax.all_to_all(jnp.stack([saved_input] * lax.axis_size('tp')), 'tp', 0, 0)  289 us
    all_gather x2, waiting for transfers between devices, in_one_piece(): out = lax.all_gather(both, axis, axis=dim, tiled=True)  128 us
    psum x2, blocking collectives, by_axis(): x = lax.psum(x, axis)  19 us
    all_to_all x1, starting transfers between devices, body(): lax.all_to_all(jnp.stack([saved_input] * lax.axis_size('tp')), 'tp', 0, 0)  15.7 us
    all_to_all x1, blocking collectives, sent_and_summed(): pieces = lax.all_to_all(cut_along(x, dim, count), axis, 0, 0, tiled=True)  14.8 us
  transfers between devices with their start and end apart: 4, of which 4 were waited for; matrix products, arithmetic and copies ran while one was open for 1% of the time, Pallas kernels for 0%

profile of v1, /device:TPU:2, one launch (start us, length us, event | category | flops | bytes accessed | tf_op | source)
XLA Modules:
  0.0 523.9 jit_solution(643318494548698429)
XLA Ops:
  7.2 1.1 copy.29
  8.3 4.3 stack.2
  12.6 15.7 %all-to-all-start = ((bf16[32,1024,128]{1,2,0:T(8,128)(2,1)}), bf16[32,1024,128]{1,2,0:T(8,128)(2,1)}, u32[]{:S(2)}, u32[]{:S(2)}) async-start(bf16[32,1024,128]{1,2,0:T(8,128)(2,1)} %stack.2), calls=%async_computation | async-start | bytes 16777216 | tf_op jit(solution)/shard_map/all_to_all | solution.py:108
  28.5 0.7 pad_maximum_fusion
  29.2 71.3 %all-gather.3.cloned.1.call-done = bf16[4096,512]{1,0:T(8,128)(2,1)} async-done(((bf16[256,512]{1,0:T(8,128)(2,1)}), bf16[4096,512]{1,0:T(8,128)(2,1)}) %all-gather.3.cloned.1.call-update) | async-done | bytes 4194320 | tf_op jit(solution)/shard_map/all_gather | solution.py:20
  100.5 288.6 %all-to-all-done = bf16[32,1024,128]{1,2,0:T(8,128)(2,1)} async-done(((bf16[32,1024,128]{1,2,0:T(8,128)(2,1)}), bf16[32,1024,128]{1,2,0:T(8,128)(2,1)}, u32[]{:S(2)}, u32[]{:S(2)}) %all-to-all-start) | async-done | bytes 8388640 | tf_op jit(solution)/shard_map/all_to_all | solution.py:108
  389.1 6.5 %fusion.4 = f32[1024,256]{0,1:T(8,128)S(1)} fusion(bf16[1024,4096]{0,1:T(8,128)(2,1)} %bitcast.1, bf16[4096,512]{1,0:T(8,128)(2,1)} %all-gather.3.cloned.1.call-done), kind=kOutput, calls=%fused_computation.4 | convolution fusion | flops 2147483648 | bytes 11534336 | tf_op jit(solution)/shard_map/dot_general | solution.py:111
  396.4 5.8 %fusion.7 = f32[1024,256]{0,1:T(8,128)S(1)} fusion(bf16[1024,4096]{0,1:T(8,128)(2,1)} %bitcast.1, bf16[4096,512]{1,0:T(8,128)(2,1)S(1)} %copy-done.1), kind=kOutput, calls=%fused_computation.5 | convolution fusion | flops 2147483648 | bytes 11534336 | tf_op jit(solution)/shard_map/dot_general | solution.py:112
  403.1 14.8 %all_to_all.15 = f32[16,16,256]{2,1,0:T(8,128)S(1)} all-to-all(f32[16,16,256]{2,1,0:T(8,128)S(1)} %bitcast.27), channel_id=1, replica_groups=mesh['fs_0'=4,'fs_1'=4,'tp'=32] {'fs_0','fs_1'}, dimensions={0} | all-to-all | bytes 524288 | tf_op jit(solution)/shard_map/all_to_all | solution.py:32
  418.6 4.8 all-to-all-start.2
  423.6 6.4 %all-to-all-done.2 = bf16[16,16,256]{2,1,0:T(8,128)(2,1)S(1)} async-done(((bf16[16,16,256]{2,1,0:T(8,128)(2,1)}), bf16[16,16,256]{2,1,0:T(8,128)(2,1)S(1)}, u32[]{:S(2)}, u32[]{:S(2)}) %all-to-all-start.2) | async-done | bytes 131104 | tf_op jit(solution)/shard_map/all_to_all | solution.py:38
  430.1 0.8 multiply_reduce_fusion
  430.9 0.8 multiply_reduce_fusion.1
  431.7 9.2 %all-reduce.1 = (f32[1]{0:T(128)}, f32[1]{0:T(128)}) all-reduce(f32[1]{0:T(128)} %bitcast.7, f32[1]{0:T(128)} %bitcast.10), channel_id=1, replica_groups=mesh['fs_0'=4,'fs_1'=4,'tp'=32] {'fs_0'}, use_global_device_ids=true, to_apply=%region_2.0 | all-reduce | flops 2 | bytes 16 | tf_op jit(solution)/shard_map/psum | solution.py:54
  440.9 9.8 %all-reduce = (f32[1]{0:T(128)}, f32[1]{0:T(128)}) all-reduce(f32[1]{0:T(128)} %get-tuple-element.32, f32[1]{0:T(128)} %get-tuple-element.33), channel_id=1, replica_groups=mesh['fs_0'=4,'fs_1'=4,'tp'=32] {'fs_1'}, use_global_device_ids=true, to_apply=%region_3.0 | all-reduce | flops 2 | bytes 16 | tf_op jit(solution)/shard_map/psum | solution.py:54
  452.1 0.7 pad_maximum_fusion.2
  453.5 0.8 copy.33
  454.2 0.8 copy.34
  455.0 0.8 copy.36
  455.7 0.8 copy.37
  456.5 56.3 %all-gather.5.cloned.1.call-done = bf16[4096,256]{0,1:T(8,128)(2,1)} async-done(((bf16[256,256]{0,1:T(8,128)(2,1)}), bf16[4096,256]{0,1:T(8,128)(2,1)}) %all-gather.5.cloned.1.call-update) | async-done | bytes 2097168 | tf_op jit(solution)/shard_map/all_gather | solution.py:20
  512.8 1.7 fusion.26
  514.5 1.3 copy.35
  515.8 1.3 copy.38
  (39 shorter events, 3.2 us)
Async XLA Ops:
  7.2 388.5 %copy-start = (bf16[1024,128]{1,0:T(8,128)(2,1)S(1)}, bf16[1024,128]{1,0:T(8,128)(2,1)}, u32[]{:S(2)}) copy-start(bf16[1024,128]{1,0:T(8,128)(2,1)} %param.12) | copy-start | bytes 786436
  12.6 15.8 %copy-start.3 = (bf16[256,256]{1,0:T(8,128)(2,1)S(1)}, bf16[256,256]{1,0:T(8,128)(2,1)}, u32[]{:S(2)}) copy-start(bf16[256,256]{1,0:T(8,128)(2,1)} %param.17) | copy-start | bytes 393220
  12.6 15.8 %copy-start.4 = (bf16[256,256]{1,0:T(8,128)(2,1)S(1)}, bf16[256,256]{1,0:T(8,128)(2,1)}, u32[]{:S(2)}) copy-start(bf16[256,256]{1,0:T(8,128)(2,1)} %param.16) | copy-start | bytes 393220
  12.6 376.5 %all-to-all-start = ((bf16[32,1024,128]{1,2,0:T(8,128)(2,1)}), bf16[32,1024,128]{1,2,0:T(8,128)(2,1)}, u32[]{:S(2)}, u32[]{:S(2)}) async-start(bf16[32,1024,128]{1,2,0:T(8,128)(2,1)} %stack.2), calls=%async_computation | async-start | bytes 16777216 | tf_op jit(solution)/shard_map/all_to_all | solution.py:108
  28.4 72.1 %all-gather.3.cloned.1.call-start = ((), (), s32[]{:S(2)}) async-start(), calls=%async_computation.3 | async-start | bytes 4456448 | tf_op jit(solution)/shard_map/all_gather | solution.py:20
  389.1 7.2 %copy-start.1 = (bf16[4096,512]{1,0:T(8,128)(2,1)S(1)}, bf16[4096,512]{1,0:T(8,128)(2,1)}, u32[]{:S(2)}) copy-start(bf16[4096,512]{1,0:T(8,128)(2,1)} %all-gather.3.cloned.1.call-done) | copy-start | bytes 12582916
  396.4 5.8 %copy-start.2 = (bf16[1024,128]{1,0:T(8,128)(2,1)S(1)}, bf16[1024,128]{1,0:T(8,128)(2,1)}, u32[]{:S(2)}) copy-start(bf16[1024,128]{1,0:T(8,128)(2,1)} %param.13) | copy-start | bytes 786436
  402.2 15.7 %copy-start.7 = (f32[16,128]{1,0:T(8,128)S(1)}, f32[16,128]{1,0:T(8,128)}, u32[]{:S(2)}) copy-start(f32[16,128]{1,0:T(8,128)} %param.21) | copy-start | bytes 24580
  402.2 15.7 %copy-start.8 = (f32[16,128]{1,0:T(8,128)S(1)}, f32[16,128]{1,0:T(8,128)}, u32[]{:S(2)}) copy-start(f32[16,128]{1,0:T(8,128)} %param.19) | copy-start | bytes 24580
  402.2 15.7 %copy-start.9 = (f32[16,128]{1,0:T(8,128)S(1)}, f32[16,128]{1,0:T(8,128)}, u32[]{:S(2)}) copy-start(f32[16,128]{1,0:T(8,128)} %param.20) | copy-start | bytes 24580
  402.2 15.7 %copy-start.10 = (f32[16,128]{1,0:T(8,128)S(1)}, f32[16,128]{1,0:T(8,128)}, u32[]{:S(2)}) copy-start(f32[16,128]{1,0:T(8,128)} %param.18) | copy-start | bytes 24580
  402.2 21.2 %copy-start.5 = (f32[256,128]{1,0:T(8,128)S(1)}, f32[256,128]{1,0:T(8,128)}, u32[]{:S(2)}) copy-start(f32[256,128]{1,0:T(8,128)} %param.14) | copy-start | bytes 393220
  402.2 21.3 %copy-start.6 = (f32[256,128]{1,0:T(8,128)S(1)}, f32[256,128]{1,0:T(8,128)}, u32[]{:S(2)}) copy-start(f32[256,128]{1,0:T(8,128)} %param.15) | copy-start | bytes 393220
  418.6 11.5 %all-to-all-start.2 = ((bf16[16,16,256]{2,1,0:T(8,128)(2,1)}), bf16[16,16,256]{2,1,0:T(8,128)(2,1)S(1)}, u32[]{:S(2)}, u32[]{:S(2)}) async-start(bf16[16,16,256]{2,1,0:T(8,128)(2,1)} %broadcast_in_dim.2), calls=%async_computation.2 | async-start | bytes 262144 | tf_op jit(solution)/shard_map/all_to_all | solution.py:38
  423.4 89.4 %all-gather.5.cloned.1.call-start = ((), (), s32[]{:S(2)}) async-start(), calls=%async_computation.4 | async-start | bytes 2228224 | tf_op jit(solution)/shard_map/all_gather | solution.py:20
Sparse Core Ops, SparseCore 0:
  32.8 67.6 all-gather.2
  453.0 59.7 all-gather.4
